TPU v7x, 32 devices: a whole 2x2x4 slice. The times are simulated.
32 devices in a mesh: grp: 2 (over y), sp: 8 (over z, core), tp: 2 (over x).
Axes of the slice: x: 2, y: 2, z: 4, core: 2. Of those that a mesh axis runs over, the one named last changes fastest.
Arguments:
- layer_input: bfloat16 [3072, 2048], P(('grp', 'sp', 'tp')), parts along dimension 0, may hold values from -6 to 6
- latent: bfloat16 [3072, 512], P(('grp', 'sp')), parts along dimension 0, may hold values from -6 to 6
- rope_key: bfloat16 [3072, 64], P(('grp', 'sp')), parts along dimension 0, may hold values from -4 to 4
- query_wide: bfloat16 [3072, 1536], P(('grp', 'sp'), 'tp'), parts along dimension 0, may hold values from -18 to 18
- query_narrow: bfloat16 [3072, 1024], P(('grp', 'sp'), 'tp'), parts along dimension 0, may hold values from -18 to 18
- key_up_wide: bfloat16 [512, 1024], P(None, 'tp'), may hold values from -0.25 to 0.25
- value_up_wide: bfloat16 [512, 1024], P(None, 'tp'), may hold values from -0.25 to 0.25
- key_up_narrow: bfloat16 [512, 512], P(None, 'tp'), may hold values from -0.25 to 0.25
- value_up_narrow: bfloat16 [512, 512], P(None, 'tp'), may hold values from -0.25 to 0.25
- out_wide: bfloat16 [1024, 2048], P('tp'), may hold values from -1.1953125 to 1.1953125
- out_narrow: bfloat16 [512, 2048], P('tp'), may hold values from -1.1953125 to 1.1953125
- norm_gain: float32 [2048], replicated, may hold values from 0.1 to 1.9
- gate_weight: bfloat16 [2048, 5632], P('sp', 'tp'), may hold values from -0.125 to 0.125
- value_weight: bfloat16 [2048, 5632], P('sp', 'tp'), may hold values from -0.125 to 0.125
- conv_weight: float32 [3, 5632], P(None, 'tp'), may hold values from -2.5 to 2.5
- down_weight: bfloat16 [5632, 2048], P('tp', 'sp'), may hold values from -0.078125 to 0.078125
Outputs:
- layer_output: bfloat16 [3072, 2048], P(('grp', 'sp', 'tp')), parts along dimension 0
There are 2 independent parts, one for each index of `grp`. A program takes and returns all parts, laid end to end along the dimension named above; an argument that names none is the same for every part. Nothing has to cross between parts.
All inputs are finite; a program needn't handle non-finite values.
Results may differ from a plain program's by a relative error of at most 0.015.
Values may be sent and summed in bfloat16 or wider, within the bound.
A program may use at most 128 MiB of HBM per device.

v0:
```python
import math
import jax
import jax.numpy as jnp
from jax import lax
from jax.sharding import PartitionSpec as P

NOPE_W = 128
NOPE_N = 64
rope_base = 10000.0
norm_eps = 1e-06


def extended(x, sides, width):
    for axis, dim in sides:
        size, length = (lax.axis_size(axis), x.shape[dim])
        up = [(i, (i + 1) % size) for i in range(size - 1)]
        down = [(j, i) for i, j in up]
        last = lax.slice_in_dim(x, length - width, length, axis=dim)
        initial = lax.slice_in_dim(x, 0, width, axis=dim)
        before = lax.ppermute(last, axis, up)
        after = lax.ppermute(initial, axis, down)
        x = jnp.concatenate([before, x, after], axis=dim)
    return x


def rope_tables(row_start, row_total, span_width):
    places = (row_start + jnp.arange(row_total, dtype=jnp.int32)).astype(jnp.float32)
    frequency = jnp.power(
        rope_base, -jnp.arange(0, span_width, 2, dtype=jnp.int32).astype(jnp.float32) / span_width
    )
    angles = places[:, None] * frequency[None, :]
    angles = jnp.concatenate([angles, angles], axis=-1)
    return (jnp.cos(angles), jnp.sin(angles))


def spin_rows(entries, cosine, sine_table):
    entries = entries.astype(jnp.float32)
    lead_half, tail_half = jnp.split(entries, 2, axis=-1)
    return entries * cosine + jnp.concatenate([-tail_half, lead_half], axis=-1) * sine_table


def prepare_queries(queries, head_count, nope_width, rot_width, cosine, sine_table):
    shaped = queries.reshape(queries.shape[0], head_count, nope_width + rot_width)
    turned = spin_rows(
        shaped[:, :, nope_width:], cosine[:, None, :], sine_table[:, None, :]
    ).astype(jnp.bfloat16)
    return (shaped[:, :, :nope_width], turned)


def start_state(row_total, head_count, value_width):
    return (
        jnp.full((row_total, head_count), -jnp.inf, jnp.float32),
        jnp.zeros((row_total, head_count), jnp.float32),
        jnp.zeros((row_total, head_count, value_width), jnp.float32),
    )


def fold_group(carried, latent_piece, rope_piece, nope_q, rope_q, key_up, value_up, score_scale):
    row_max, row_sum, weighted = carried
    piece_rows = latent_piece.shape[0]
    head_count = nope_q.shape[1]
    key_rows = jnp.dot(latent_piece, key_up, preferred_element_type=jnp.float32).astype(
        jnp.bfloat16
    )
    key_rows = key_rows.reshape(piece_rows, head_count, -1)
    value_rows = jnp.dot(latent_piece, value_up, preferred_element_type=jnp.float32).astype(
        jnp.bfloat16
    )
    value_rows = value_rows.reshape(piece_rows, head_count, -1)
    scores = jnp.einsum("qhd,khd->qhk", nope_q, key_rows, preferred_element_type=jnp.float32)
    scores = (
        scores + jnp.einsum("qhd,kd->qhk", rope_q, rope_piece, preferred_element_type=jnp.float32)
    ) * score_scale
    new_max = jnp.max(scores, axis=-1)
    shrink = jnp.exp(row_max - new_max)
    weights = jnp.exp(scores - new_max[:, :, None])
    row_sum = row_sum * shrink + jnp.sum(weights, axis=-1)
    weighted = weighted * shrink[:, :, None] + jnp.einsum(
        "qhk,khd->qhd", weights.astype(jnp.bfloat16), value_rows, preferred_element_type=jnp.float32
    )
    return (new_max, row_sum, weighted)


def finish_group(carried):
    row_max, row_sum, weighted = carried
    return (weighted / row_sum[:, :, None]).reshape(weighted.shape[0], -1).astype(jnp.bfloat16)


def on_device(
    layer_input,
    latent,
    rope_key,
    query_wide,
    query_narrow,
    key_up_wide,
    value_up_wide,
    key_up_narrow,
    value_up_narrow,
    out_wide,
    out_narrow,
    norm_gain,
    gate_weight,
    value_weight,
    conv_weight,
    down_weight,
):
    seq_rows = latent.shape[0]
    rot_width = rope_key.shape[1]
    row_start = lax.axis_index("sp") * seq_rows
    cosine, sine_table = rope_tables(row_start, seq_rows, rot_width)
    turned_key = spin_rows(rope_key, cosine, sine_table).astype(jnp.bfloat16)
    wide_heads = key_up_wide.shape[1] // NOPE_W
    narrow_heads = key_up_narrow.shape[1] // NOPE_N
    wide_nope, wide_rope = prepare_queries(
        query_wide, wide_heads, NOPE_W, rot_width, cosine, sine_table
    )
    narrow_nope, narrow_rope = prepare_queries(
        query_narrow, narrow_heads, NOPE_N, rot_width, cosine, sine_table
    )
    wide_scale = 1.0 / math.sqrt(NOPE_W + rot_width)
    narrow_scale = 1.0 / math.sqrt(NOPE_N + rot_width)
    initial = (
        start_state(seq_rows, wide_heads, value_up_wide.shape[1] // wide_heads),
        start_state(seq_rows, narrow_heads, value_up_narrow.shape[1] // narrow_heads),
    )
    latent_piece = lax.all_gather(latent, "sp", axis=0, tiled=True)
    rope_piece = lax.all_gather(turned_key, "sp", axis=0, tiled=True)
    wide_state = fold_group(
        initial[0],
        latent_piece,
        rope_piece,
        wide_nope,
        wide_rope,
        key_up_wide,
        value_up_wide,
        wide_scale,
    )
    narrow_state = fold_group(
        initial[1],
        latent_piece,
        rope_piece,
        narrow_nope,
        narrow_rope,
        key_up_narrow,
        value_up_narrow,
        narrow_scale,
    )
    wide_out = finish_group(wide_state)
    narrow_out = finish_group(narrow_state)
    attended = lax.psum_scatter(
        (
            jnp.dot(wide_out, out_wide, preferred_element_type=jnp.float32)
            + jnp.dot(narrow_out, out_narrow, preferred_element_type=jnp.float32)
        ).astype(jnp.bfloat16),
        "tp",
        scatter_dimension=0,
        tiled=True,
    ).astype(jnp.float32)
    middle = (layer_input.astype(jnp.float32) + attended).astype(jnp.bfloat16)
    middle_full = middle.astype(jnp.float32)
    normed = middle_full * lax.rsqrt(
        jnp.mean(middle_full * middle_full, axis=-1, keepdims=True) + norm_eps
    )
    normed = (normed * norm_gain).astype(jnp.bfloat16)
    all_rows = lax.all_gather(normed, "tp", axis=0, tiled=True)
    hidden_width = gate_weight.shape[1]
    stacked = jnp.concatenate(
        (
            lax.all_gather(gate_weight, "sp", axis=0, tiled=True),
            lax.all_gather(value_weight, "sp", axis=0, tiled=True),
        ),
        axis=1,
    )
    both_pre = jnp.dot(all_rows, stacked, preferred_element_type=jnp.float32)
    gate_pre = both_pre[:, :hidden_width]
    value_pre = both_pre[:, hidden_width:]
    padded = extended(gate_pre.astype(jnp.bfloat16), (("sp", 0),), 1)
    conv_gate = jnp.zeros(gate_pre.shape, jnp.float32)
    for kernel_tap in range(conv_weight.shape[0]):
        conv_gate = conv_gate + conv_weight[kernel_tap] * padded[
            kernel_tap : kernel_tap + seq_rows
        ].astype(jnp.float32)
    hidden = (jax.nn.silu(conv_gate) * value_pre).astype(jnp.bfloat16)
    terms = jnp.dot(
        hidden,
        lax.all_gather(down_weight, "sp", axis=1, tiled=True),
        preferred_element_type=jnp.float32,
    )
    summed = lax.psum_scatter(
        terms.astype(jnp.bfloat16), "tp", scatter_dimension=0, tiled=True
    ).astype(jnp.float32)
    return (middle_full + summed).astype(jnp.bfloat16)


def solution(mesh):
    in_specs = (
        P(("grp", "sp", "tp"), None),
        P(("grp", "sp"), None),
        P(("grp", "sp"), None),
        P(("grp", "sp"), "tp"),
        P(("grp", "sp"), "tp"),
        P(None, "tp"),
        P(None, "tp"),
        P(None, "tp"),
        P(None, "tp"),
        P("tp", None),
        P("tp", None),
        P(),
        P("sp", "tp"),
        P("sp", "tp"),
        P(None, "tp"),
        P("tp", "sp"),
    )
    out_specs = P(("grp", "sp", "tp"), None)
    return jax.shard_map(
        on_device, mesh=mesh, in_specs=in_specs, out_specs=out_specs, check_vma=False
    )
```

profile of v0, /device:TPU:0, one launch (start us, length us, event | category | flops | bytes accessed | tf_op | source)
XLA Modules:
  0.0 431.2 jit_solution(12649562637547204300)
XLA Ops:
  6.5 0.7 all-gather.6.cloned.1.call-update
  7.3 0.8 convert_element_type.108
  8.1 0.7 split.27
  8.8 1.0 reshape.120
  9.8 1.3 reshape.117
  11.2 0.9 fusion.70
  12.2 0.8 copy.37
  12.9 0.7 copy.38
  13.7 16.9 %all-gather = bf16[8,192,64]{1,2,0:T(8,128)(2,1)S(1)} all-gather(bf16[1,192,64]{1,2,0:T(8,128)(2,1)S(1)} %get-tuple-element.19), channel_id=1, replica_groups=mesh['grp'=2,'sp'=8,'tp'=2] {'sp'}, dimensions={0}, use_global_device_ids=true | all-gather | bytes 221184 | tf_op jit(solution)/shard_map/all_gather | solution.py:127
  31.2 0.5 slice_negate_fusion
  32.0 0.7 fusion.59
  32.7 5.7 %all-gather.6.cloned.1.call-done = bf16[1536,512]{1,0:T(8,128)(2,1)} async-done(((bf16[192,512]{1,0:T(8,128)(2,1)}), bf16[1536,512]{1,0:T(8,128)(2,1)}) %all-gather.6.cloned.1.call-update) | async-done | bytes 1572880 | tf_op jit(solution)/shard_map/all_gather | solution.py:126
  38.4 2.0 convolution_convert_fusion.3
  40.4 0.7 fusion.63
  41.2 0.9 fusion.81
  42.1 0.8 fusion.8
  42.9 0.6 copy-done.2
  43.6 1.0 convolution_convert_fusion.1
  44.6 0.8 fusion.65
  45.4 0.9 fusion.80
  46.3 0.8 fusion.6
  47.1 0.2 copy-done.13
  47.3 1.0 convolution_convert_fusion
  48.3 0.9 fusion.49
  49.3 0.6 fusion.60
  49.9 0.4 copy-done.9
  50.2 0.6 convolution_convert_fusion.2
  50.9 1.0 fusion.33
  51.8 0.2 copy-done.6
  52.1 1.3 fusion.10
  53.5 0.7 all-gather.10.cloned.1.call-update
  54.2 0.5 all-gather.8.cloned.1.call-update
  54.8 0.5 all-gather.12.cloned.1.call-update
  55.6 14.8 %reduce-scatter.3.cloned.1.call-done = bf16[96,2048]{1,0:T(8,128)(2,1)} async-done(((bf16[192,2048]{1,0:T(8,128)(2,1)}), bf16[96,2048]{1,0:T(8,128)(2,1)}) %reduce-scatter.3.cloned.1.call-update) | async-done | bytes 393232 | tf_op jit(solution)/shard_map/reduce_scatter | solution.py:150
  70.3 1.2 fusion.52
  71.6 1.2 fusion.54
  72.8 11.3 %all_gather.20 = bf16[192,2048]{1,0:T(8,128)(2,1)S(1)} all-gather(bf16[96,2048]{1,0:T(8,128)(2,1)S(1)} %fusion.54), channel_id=1, replica_groups=mesh['grp'=2,'sp'=8,'tp'=2] {'tp'}, dimensions={0}, use_global_device_ids=true | all-gather | bytes 1179648 | tf_op jit(solution)/shard_map/all_gather | solution.py:165
  84.1 96.0 %all-gather.10.cloned.1.call-done = bf16[2048,2816]{1,0:T(8,128)(2,1)} async-done(((bf16[256,2816]{1,0:T(8,128)(2,1)}), bf16[2048,2816]{1,0:T(8,128)(2,1)}) %all-gather.10.cloned.1.call-update) | async-done | bytes 11534352 | tf_op jit(solution)/shard_map/all_gather | solution.py:170
  180.1 107.8 %all-gather.8.cloned.1.call-done = bf16[2048,2816]{1,0:T(8,128)(2,1)} async-done(((bf16[256,2816]{1,0:T(8,128)(2,1)}), bf16[2048,2816]{1,0:T(8,128)(2,1)}) %all-gather.8.cloned.1.call-update) | async-done | bytes 11534352 | tf_op jit(solution)/shard_map/all_gather | solution.py:169
  287.9 13.6 %fusion.82 = (bf16[192,5632]{1,0:T(8,128)(2,1)}, f32[192,5632]{1,0:T(8,128)}) fusion(bf16[192,2048]{1,0:T(8,128)(2,1)S(1)} %all_gather.20, bf16[2048,2816]{1,0:T(8,128)(2,1)} %all-gather.10.cloned.1.call-done, bf16[2048,2816]{1,0:T(8,128)(2,1)} %all-gather.8.cloned.1.call-done), kind=kOutput, calls=%fused_computation.96 | convolution fusion | flops 4476403712 | bytes 30343168 | tf_op jit(solution)/shard_map/dot_general | solution.py:174
  301.5 0.8 fusion.79
  302.4 2.1 collective-permute-start
  304.5 1.3 collective-permute-start.1
  305.9 2.3 slice.62
  308.2 88.0 %all-gather.12.cloned.1.call-done = bf16[2816,2048]{1,0:T(8,128)(2,1)} async-done(((bf16[2816,256]{1,0:T(8,128)(2,1)}), bf16[2816,2048]{1,0:T(8,128)(2,1)}) %all-gather.12.cloned.1.call-update) | async-done | bytes 11534352 | tf_op jit(solution)/shard_map/all_gather | solution.py:186
  396.2 10.3 %convolution_convert_fusion.4 = bf16[192,2048]{1,0:T(8,128)(2,1)} fusion(bf16[2816,2048]{1,0:T(8,128)(2,1)} %all-gather.12.cloned.1.call-done, f32[192,5632]{1,0:T(8,128)} %get-tuple-element.30, bf16[192,2816]{1,0:T(8,128)(2,1)} %slice.62, bf16[1,2816]{1,0:T(2,128)(2,1)S(1)} %collective-permute-done.1, bf16[1,2816]{1,0:T(2,128)(2,1)S(1)} %collective-permute-done, ...), kind=kOutput, calls=%fused_computation.20 | convolution fusion | flops 2225799168 | bytes 15609856 | tf_op jit(solution)/shard_map/dot_general | solution.py:184
  406.6 15.8 %reduce-scatter.5.cloned.1.call-done = bf16[96,2048]{1,0:T(8,128)(2,1)} async-done(((bf16[192,2048]{1,0:T(8,128)(2,1)}), bf16[96,2048]{1,0:T(8,128)(2,1)}) %reduce-scatter.5.cloned.1.call-update) | async-done | bytes 393232 | tf_op jit(solution)/shard_map/reduce_scatter | solution.py:189
  422.4 1.9 fusion.55
  (47 shorter events, 1.6 us)
Async XLA Ops:
  6.5 42.7 %copy-start = (bf16[512,2048]{1,0:T(8,128)(2,1)S(1)}, bf16[512,2048]{1,0:T(8,128)(2,1)}, u32[]{:S(2)}) copy-start(bf16[512,2048]{1,0:T(8,128)(2,1)} %param.25) | copy-start | bytes 6291460
  6.5 31.9 %all-gather.6.cloned.1.call-start = ((), (), s32[]{:S(2)}) async-start(), calls=%async_computation.2 | async-start | bytes 1769472 | tf_op jit(solution)/shard_map/all_gather | solution.py:126
  7.3 63.1 %reduce-scatter.3.cloned.1.call-start = ((), (), s32[]{:S(2)}) async-start(), calls=%async_computation.3 | async-start | bytes 1179648 | tf_op jit(solution)/shard_map/reduce_scatter | solution.py:150
  11.1 20.6 %copy-start.5 = (bf16[192,4,192]{2,1,0:T(4,128)(2,1)}, bf16[192,4,192]{2,1,0:T(4,128)(2,1)S(1)}, u32[]{:S(2)}) copy-start(bf16[192,4,192]{2,1,0:T(4,128)(2,1)S(1)} %reshape.117) | copy-start | bytes 884740
  31.0 0.9 copy-start.7
  31.0 0.9 copy-start.8
  42.1 1.4 copy-start.2
  42.1 1.5 copy-start.12
  43.6 1.0 slice-start
  46.3 1.0 copy-start.13
  49.3 1.0 copy-start.9
  50.9 1.2 copy-start.6
  53.4 16.9 %copy-start.3 = (bf16[96,2048]{1,0:T(8,128)(2,1)S(1)}, bf16[96,2048]{1,0:T(8,128)(2,1)}, u32[]{:S(2)}) copy-start(bf16[96,2048]{1,0:T(8,128)(2,1)} %param.16) | copy-start | bytes 1179652
  53.4 126.6 %all-gather.10.cloned.1.call-start = ((), (), s32[]{:S(2)}) async-start(), calls=%async_computation.5 | async-start | bytes 12976128 | tf_op jit(solution)/shard_map/all_gather | solution.py:170
  54.2 17.4 %copy-start.11 = (f32[2048]{0:T(1024)S(1)}, f32[2048]{0:T(1024)}, u32[]{:S(2)}) copy-start(f32[2048]{0:T(1024)} %param.27) | copy-start | bytes 24580
  54.2 233.7 %all-gather.8.cloned.1.call-start = ((), (), s32[]{:S(2)}) async-start(), calls=%async_computation.4 | async-start | bytes 12976128 | tf_op jit(solution)/shard_map/all_gather | solution.py:169
  54.8 341.5 %all-gather.12.cloned.1.call-start = ((), (), s32[]{:S(2)}) async-start(), calls=%async_computation.6 | async-start | bytes 12976128 | tf_op jit(solution)/shard_map/all_gather | solution.py:186
  55.4 367.1 %reduce-scatter.5.cloned.1.call-start = ((), (), s32[]{:S(2)}) async-start(), calls=%async_computation.7 | async-start | bytes 1179648 | tf_op jit(solution)/shard_map/reduce_scatter | solution.py:189
  84.1 221.7 %copy-start.10 = (f32[3,2816]{1,0:T(4,128)S(1)}, f32[3,2816]{1,0:T(4,128)}, u32[]{:S(2)}) copy-start(f32[3,2816]{1,0:T(4,128)} %param.30) | copy-start | bytes 101380
  302.4 93.9 %collective-permute-start = (bf16[1,2816]{1,0:T(2,128)(2,1)S(1)}, bf16[1,2816]{1,0:T(2,128)(2,1)S(1)}, u32[]{:S(2)}, u32[]{:S(2)}) collective-permute-start(bf16[1,2816]{1,0:T(2,128)(2,1)S(1)} %get-tuple-element.8), channel_id=1, source_target_pairs={{0,2},{2,4},{4,6},{6,8},{8,10},{10,12},{12,14},{1,3},{3,5},{5,7},{... | collective-permute-start | bytes 16904 | tf_op jit(solution)/shard_map/ppermute | solution.py:20
  304.5 91.7 %collective-permute-start.1 = (bf16[1,2816]{1,0:T(2,128)(2,1)S(1)}, bf16[1,2816]{1,0:T(2,128)(2,1)S(1)}, u32[]{:S(2)}, u32[]{:S(2)}) collective-permute-start(bf16[1,2816]{1,0:T(2,128)(2,1)S(1)} %get-tuple-element.9), channel_id=1, source_target_pairs={{2,0},{4,2},{6,4},{8,6},{10,8},{12,10},{14,12},{3,1},{5,3},{7,5},{... | collective-permute-start | bytes 16904 | tf_op jit(solution)/shard_map/ppermute | solution.py:21
  396.2 26.2 %copy-start.4 = (bf16[96,2048]{1,0:T(8,128)(2,1)S(1)}, bf16[96,2048]{1,0:T(8,128)(2,1)}, u32[]{:S(2)}) copy-start(bf16[96,2048]{1,0:T(8,128)(2,1)} %reduce-scatter.3.cloned.1.call-done) | copy-start | bytes 1179652
  396.2 28.1 %copy-start.1 = (bf16[512,2048]{1,0:T(8,128)(2,1)S(1)}, bf16[512,2048]{1,0:T(8,128)(2,1)}, u32[]{:S(2)}) copy-start(bf16[512,2048]{1,0:T(8,128)(2,1)} %param.25) | copy-start | bytes 6291460
Sparse Core Ops, SparseCore 0:
  9.0 29.3 all-gather.5
  53.6 16.7 reduce-scatter.2
  72.0 108.0 all-gather.9
  181.6 106.2 all-gather.7
  289.3 106.8 all-gather.11
  406.7 15.6 reduce-scatter.4
where the time goes:
time: 432 us; the launch traced here: 431 us
  waiting for transfers between devices  331 us (77%)
  matrix products  35.7 us (8%)
  blocking collectives  28.3 us (7%)
  between operations  13.7 us (3%)
  local copies, waits for them, and re-layouts  10 us (2%)
  other arithmetic  9.03 us (2%)
    all_gather x1, waiting for transfers between devices, on_device(): lax.all_gather(gate_weight, 'sp', axis=0, tiled=True)  108 us
    all_gather x1, waiting for transfers between devices, on_device(): lax.all_gather(value_weight, 'sp', axis=0, tiled=True)  96 us
    all_gather x1, waiting for transfers between devices, on_device(): lax.all_gather(down_weight, 'sp', axis=1, tiled=True)  88 us
    all_gather x1, blocking collectives, on_device(): rope_piece = lax.all_gather(turned_key, 'sp', axis=0, tiled=True)  16.9 us
    reduce_scatter x1, waiting for transfers between devices, on_device(): lax.psum_scatter(terms.astype(jnp.bfloat16), 'tp', scatter_dimension=0, t...  15.8 us
    reduce_scatter x1, waiting for transfers between devices, on_device(): lax.psum_scatter((jnp.dot(wide_out, out_wide, preferred_element_type=jnp....  14.8 us
    dot_general x1, matrix products, on_device(): both_pre = jnp.dot(all_rows, stacked, preferred_element_type=jnp.float32)  13.6 us
    all_gather x1, blocking collectives, on_device(): all_rows = lax.all_gather(normed, 'tp', axis=0, tiled=True)  11.3 us
  transfers between devices with their start and end apart: 8, of which 6 were waited for; matrix products, arithmetic and copies ran while one was open for 6% of the time, Pallas kernels for 0%

commit v1 on v0

--- a/solution.py
+++ b/solution.py
@@ -183,7 +183,7 @@
     hidden = (jax.nn.silu(conv_gate) * value_pre).astype(jnp.bfloat16)
     terms = jnp.dot(
         hidden,
-        lax.all_gather(down_weight, "sp", axis=1, tiled=True),
+        jnp.concatenate(lax.all_gather(down_weight, "sp"), axis=1),
         preferred_element_type=jnp.float32,
     )
     summed = lax.psum_scatter(

time: 432 us -> 448 us (1.037)
  local copies, waits for them, and re-layouts: 10 us -> 25.1 us
    reshape x0 -> x1, local copies, waits for them, and re-layouts: none -> 15.1 us  [on_device(): jnp.concatenate(lax.all_gather(down_weight, 'sp'), axis=1)]
  transfers between devices with their start and end apart: 8 -> 8, of which waited for: 6 -> 6; matrix products, arithmetic and copies ran while one was open for 6% -> 9% of each run, Pallas kernels for 0% -> 0%
where the time goes in v1:
time: 448 us; the launch traced here: 447 us
  waiting for transfers between devices  330 us (74%)
  matrix products  36.6 us (8%)
  blocking collectives  28.3 us (6%)
  local copies, waits for them, and re-layouts  25.1 us (6%)
  between operations  13.8 us (3%)
  other arithmetic  9.03 us (2%)
    all_gather x1, waiting for transfers between devices, on_device(): lax.all_gather(gate_weight, 'sp', axis=0, tiled=True)  108 us
    all_gather x1, waiting for transfers between devices, on_device(): lax.all_gather(value_weight, 'sp', axis=0, tiled=True)  96 us
    all_gather x1, waiting for transfers between devices, on_device(): lax.all_gather(down_weight, 'sp')  87.6 us
    all_gather x1, blocking collectives, on_device(): rope_piece = lax.all_gather(turned_key, 'sp', axis=0, tiled=True)  16.9 us
    reduce_scatter x1, waiting for transfers between devices, on_device(): lax.psum_scatter(terms.astype(jnp.bfloat16), 'tp', scatter_dimension=0, t...  15.9 us
    reshape x1, local copies, waits for them, and re-layouts, on_device(): jnp.concatenate(lax.all_gather(down_weight, 'sp'), axis=1)  15.1 us
    reduce_scatter x1, waiting for transfers between devices, on_device(): lax.psum_scatter((jnp.dot(wide_out, out_wide, preferred_element_type=jnp....  14.8 us
    dot_general x1, matrix products, on_device(): both_pre = jnp.dot(all_rows, stacked, preferred_element_type=jnp.float32)  13.6 us
  transfers between devices with their start and end apart: 8, of which 6 were waited for; matrix products, arithmetic and copies ran while one was open for 9% of the time, Pallas kernels for 0%

profile of v1, /device:TPU:0, one launch (start us, length us, event | category | flops | bytes accessed | tf_op | source)
XLA Modules:
  0.0 446.9 jit_solution(894227826116372541)
XLA Ops:
  6.5 0.7 all-gather.7.cloned.1.call-update
  7.3 0.8 convert_element_type.108
  8.1 0.7 split.27
  8.8 1.0 reshape.126
  9.8 1.3 reshape.123
  11.2 0.9 fusion.70
  12.2 0.8 copy.48
  12.9 0.7 copy.49
  13.7 16.9 %all-gather.1 = bf16[8,192,64]{1,2,0:T(8,128)(2,1)S(1)} all-gather(bf16[1,192,64]{1,2,0:T(8,128)(2,1)S(1)} %get-tuple-element.19), channel_id=1, replica_groups=mesh['grp'=2,'sp'=8,'tp'=2] {'sp'}, dimensions={0}, use_global_device_ids=true | all-gather | bytes 221184 | tf_op jit(solution)/shard_map/all_gather | solution.py:127
  31.2 0.5 slice_negate_fusion
  32.0 0.7 fusion.59
  32.7 5.7 %all-gather.7.cloned.1.call-done = bf16[1536,512]{1,0:T(8,128)(2,1)} async-done(((bf16[192,512]{1,0:T(8,128)(2,1)}), bf16[1536,512]{1,0:T(8,128)(2,1)}) %all-gather.7.cloned.1.call-update) | async-done | bytes 1572880 | tf_op jit(solution)/shard_map/all_gather | solution.py:126
  38.4 2.0 convolution_convert_fusion.3
  40.4 0.7 fusion.63
  41.2 0.9 fusion.81
  42.1 0.8 fusion.8
  42.9 0.6 copy-done.2
  43.6 1.0 convolution_convert_fusion.1
  44.6 0.8 fusion.65
  45.4 0.9 fusion.80
  46.3 0.8 fusion.6
  47.3 1.0 convolution_convert_fusion
  48.3 0.9 fusion.49
  49.3 0.6 fusion.60
  49.9 0.4 copy-done.9
  50.2 0.6 convolution_convert_fusion.2
  50.9 1.0 fusion.33
  51.8 0.2 copy-done.6
  52.1 1.3 fusion.10
  53.5 0.7 all-gather.11.cloned.1.call-update
  54.2 0.5 all-gather.9.cloned.1.call-update
  54.8 0.5 all-gather.13.cloned.1.call-update
  55.6 14.8 %reduce-scatter.3.cloned.1.call-done = bf16[96,2048]{1,0:T(8,128)(2,1)} async-done(((bf16[192,2048]{1,0:T(8,128)(2,1)}), bf16[96,2048]{1,0:T(8,128)(2,1)}) %reduce-scatter.3.cloned.1.call-update) | async-done | bytes 393232 | tf_op jit(solution)/shard_map/reduce_scatter | solution.py:150
  70.3 1.2 fusion.52
  71.6 1.2 fusion.54
  72.8 11.3 %all_gather.23 = bf16[192,2048]{1,0:T(8,128)(2,1)S(1)} all-gather(bf16[96,2048]{1,0:T(8,128)(2,1)S(1)} %fusion.54), channel_id=1, replica_groups=mesh['grp'=2,'sp'=8,'tp'=2] {'tp'}, dimensions={0}, use_global_device_ids=true | all-gather | bytes 1179648 | tf_op jit(solution)/shard_map/all_gather | solution.py:165
  84.1 96.0 %all-gather.11.cloned.1.call-done = bf16[2048,2816]{1,0:T(8,128)(2,1)} async-done(((bf16[256,2816]{1,0:T(8,128)(2,1)}), bf16[2048,2816]{1,0:T(8,128)(2,1)}) %all-gather.11.cloned.1.call-update) | async-done | bytes 11534352 | tf_op jit(solution)/shard_map/all_gather | solution.py:170
  180.1 107.8 %all-gather.9.cloned.1.call-done = bf16[2048,2816]{1,0:T(8,128)(2,1)} async-done(((bf16[256,2816]{1,0:T(8,128)(2,1)}), bf16[2048,2816]{1,0:T(8,128)(2,1)}) %all-gather.9.cloned.1.call-update) | async-done | bytes 11534352 | tf_op jit(solution)/shard_map/all_gather | solution.py:169
  287.9 13.6 %fusion.82 = (bf16[192,5632]{1,0:T(8,128)(2,1)}, f32[192,5632]{1,0:T(8,128)}) fusion(bf16[192,2048]{1,0:T(8,128)(2,1)S(1)} %all_gather.23, bf16[2048,2816]{1,0:T(8,128)(2,1)} %all-gather.11.cloned.1.call-done, bf16[2048,2816]{1,0:T(8,128)(2,1)} %all-gather.9.cloned.1.call-done), kind=kOutput, calls=%fused_computation.96 | convolution fusion | flops 4476403712 | bytes 30343168 | tf_op jit(solution)/shard_map/dot_general | solution.py:174
  301.5 0.8 fusion.79
  302.3 2.2 collective-permute-start
  304.5 1.3 collective-permute-start.1
  305.9 2.3 slice.62
  308.2 87.6 %all-gather.13.cloned.1.call-done = bf16[22528,256]{1,0:T(8,128)(2,1)} async-done(((bf16[2816,256]{1,0:T(8,128)(2,1)}), bf16[22528,256]{1,0:T(8,128)(2,1)}) %all-gather.13.cloned.1.call-update) | async-done | bytes 11534352 | tf_op jit(solution)/shard_map/all_gather | solution.py:186
  395.8 15.1 %copy.56 = bf16[2816,8,256]{0,2,1:T(8,128)(2,1)} copy(bf16[2816,8,256]{2,0,1:T(8,128)(2,1)} %bitcast.63) | data formatting | bytes 23068672 | tf_op jit(solution)/shard_map/reshape | solution.py:186
  410.9 11.2 %convolution_convert_fusion.4 = bf16[192,2048]{1,0:T(8,128)(2,1)} fusion(bf16[2816,2048]{0,1:T(8,128)(2,1)} %bitcast.64, f32[192,5632]{1,0:T(8,128)} %get-tuple-element.30, bf16[192,2816]{1,0:T(8,128)(2,1)} %slice.62, bf16[1,2816]{1,0:T(2,128)(2,1)S(1)} %collective-permute-done.1, bf16[1,2816]{1,0:T(2,128)(2,1)S(1)} %collective-permute-done, ...), kind=kOutput, calls=%fused_computation.20 | convolution fusion | flops 2225799168 | bytes 15609856 | tf_op jit(solution)/shard_map/dot_general | solution.py:184
  422.2 15.9 %reduce-scatter.5.cloned.1.call-done = bf16[96,2048]{1,0:T(8,128)(2,1)} async-done(((bf16[192,2048]{1,0:T(8,128)(2,1)}), bf16[96,2048]{1,0:T(8,128)(2,1)}) %reduce-scatter.5.cloned.1.call-update) | async-done | bytes 393232 | tf_op jit(solution)/shard_map/reduce_scatter | solution.py:189
  438.1 1.9 fusion.55
  (48 shorter events, 1.9 us)
Async XLA Ops:
  6.5 42.7 %copy-start = (bf16[512,2048]{1,0:T(8,128)(2,1)S(1)}, bf16[512,2048]{1,0:T(8,128)(2,1)}, u32[]{:S(2)}) copy-start(bf16[512,2048]{1,0:T(8,128)(2,1)} %param.25) | copy-start | bytes 6291460
  6.5 31.9 %all-gather.7.cloned.1.call-start = ((), (), s32[]{:S(2)}) async-start(), calls=%async_computation.2 | async-start | bytes 1769472 | tf_op jit(solution)/shard_map/all_gather | solution.py:126
  7.3 63.1 %reduce-scatter.3.cloned.1.call-start = ((), (), s32[]{:S(2)}) async-start(), calls=%async_computation.3 | async-start | bytes 1179648 | tf_op jit(solution)/shard_map/reduce_scatter | solution.py:150
  11.1 20.6 %copy-start.5 = (bf16[192,4,192]{2,1,0:T(4,128)(2,1)}, bf16[192,4,192]{2,1,0:T(4,128)(2,1)S(1)}, u32[]{:S(2)}) copy-start(bf16[192,4,192]{2,1,0:T(4,128)(2,1)S(1)} %reshape.123) | copy-start | bytes 884740
  31.0 0.9 copy-start.7
  31.0 0.9 copy-start.8
  42.1 1.4 copy-start.2
  42.1 1.5 copy-start.12
  43.6 1.0 slice-start
  46.3 1.0 copy-start.13
  49.3 1.0 copy-start.9
  50.9 1.2 copy-start.6
  53.4 16.9 %copy-start.3 = (bf16[96,2048]{1,0:T(8,128)(2,1)S(1)}, bf16[96,2048]{1,0:T(8,128)(2,1)}, u32[]{:S(2)}) copy-start(bf16[96,2048]{1,0:T(8,128)(2,1)} %param.16) | copy-start | bytes 1179652
  53.4 126.6 %all-gather.11.cloned.1.call-start = ((), (), s32[]{:S(2)}) async-start(), calls=%async_computation.5 | async-start | bytes 12976128 | tf_op jit(solution)/shard_map/all_gather | solution.py:170
  54.2 17.4 %copy-start.11 = (f32[2048]{0:T(1024)S(1)}, f32[2048]{0:T(1024)}, u32[]{:S(2)}) copy-start(f32[2048]{0:T(1024)} %param.27) | copy-start | bytes 24580
  54.2 233.7 %all-gather.9.cloned.1.call-start = ((), (), s32[]{:S(2)}) async-start(), calls=%async_computation.4 | async-start | bytes 12976128 | tf_op jit(solution)/shard_map/all_gather | solution.py:169
  54.8 341.0 %all-gather.13.cloned.1.call-start = ((), (), s32[]{:S(2)}) async-start(), calls=%async_computation.7 | async-start | bytes 12976128 | tf_op jit(solution)/shard_map/all_gather | solution.py:186
  55.4 382.8 %reduce-scatter.5.cloned.1.call-start = ((), (), s32[]{:S(2)}) async-start(), calls=%async_computation.6 | async-start | bytes 1179648 | tf_op jit(solution)/shard_map/reduce_scatter | solution.py:189
  84.1 221.7 %copy-start.10 = (f32[3,2816]{1,0:T(4,128)S(1)}, f32[3,2816]{1,0:T(4,128)}, u32[]{:S(2)}) copy-start(f32[3,2816]{1,0:T(4,128)} %param.30) | copy-start | bytes 101380
  302.3 108.6 %collective-permute-start = (bf16[1,2816]{1,0:T(2,128)(2,1)S(1)}, bf16[1,2816]{1,0:T(2,128)(2,1)S(1)}, u32[]{:S(2)}, u32[]{:S(2)}) collective-permute-start(bf16[1,2816]{1,0:T(2,128)(2,1)S(1)} %get-tuple-element.8), channel_id=1, source_target_pairs={{0,2},{2,4},{4,6},{6,8},{8,10},{10,12},{12,14},{1,3},{3,5},{5,7},{... | collective-permute-start | bytes 16904 | tf_op jit(solution)/shard_map/ppermute | solution.py:20
  304.5 106.4 %collective-permute-start.1 = (bf16[1,2816]{1,0:T(2,128)(2,1)S(1)}, bf16[1,2816]{1,0:T(2,128)(2,1)S(1)}, u32[]{:S(2)}, u32[]{:S(2)}) collective-permute-start(bf16[1,2816]{1,0:T(2,128)(2,1)S(1)} %get-tuple-element.9), channel_id=1, source_target_pairs={{2,0},{4,2},{6,4},{8,6},{10,8},{12,10},{14,12},{3,1},{5,3},{7,5},{... | collective-permute-start | bytes 16904 | tf_op jit(solution)/shard_map/ppermute | solution.py:21
  410.9 27.2 %copy-start.4 = (bf16[96,2048]{1,0:T(8,128)(2,1)S(1)}, bf16[96,2048]{1,0:T(8,128)(2,1)}, u32[]{:S(2)}) copy-start(bf16[96,2048]{1,0:T(8,128)(2,1)} %reduce-scatter.3.cloned.1.call-done) | copy-start | bytes 1179652
  410.9 29.1 %copy-start.1 = (bf16[512,2048]{1,0:T(8,128)(2,1)S(1)}, bf16[512,2048]{1,0:T(8,128)(2,1)}, u32[]{:S(2)}) copy-start(bf16[512,2048]{1,0:T(8,128)(2,1)} %param.25) | copy-start | bytes 6291460
Sparse Core Ops, SparseCore 0:
  9.0 29.3 all-gather.6
  53.6 16.7 reduce-scatter.2
  72.0 108.0 all-gather.10
  181.6 106.2 all-gather.8
  289.4 106.3 all-gather.12
  422.3 15.7 reduce-scatter.4
